TPU v7x, 32 devices: a whole 2x2x4 slice. The times are simulated.
32 devices in a mesh: ep: 8 (over z, y), tp: 4 (over x, core).
Axes of the slice: x: 2, y: 2, z: 4, core: 2. Of those that a mesh axis runs over, the one named last changes fastest.
Arguments:
- tokens: bfloat16 [128, 1024], P('ep'), may hold values from -6 to 6
- attn_gain: float32 [1024], replicated, may hold values from 0.1 to 1.9
- q_down: bfloat16 [1024, 512], P(None, 'tp'), may hold values from -0.1875 to 0.1875
- kv_down: bfloat16 [1024, 512], P(None, 'tp'), may hold values from -0.1875 to 0.1875
- rope_down: bfloat16 [1024, 32], replicated, may hold values from -0.1875 to 0.1875
- q_latent_gain: float32 [512], replicated, may hold values from 0.1 to 1.9
- kv_latent_gain: float32 [512], replicated, may hold values from 0.1 to 1.9
- q_up: bfloat16 [512, 768], P(None, 'tp'), may hold values from -0.25 to 0.25
- query_gain: float32 [8, 96], P('tp'), may hold values from 0.4 to 48
- key_up: bfloat16 [512, 512], P(None, 'tp'), may hold values from -0.25 to 0.25
- value_up: bfloat16 [512, 512], P(None, 'tp'), may hold values from -0.25 to 0.25
- attn_out: bfloat16 [512, 1024], P('tp'), may hold values from -0.25 to 0.25
- cache_latent: bfloat16 [128, 512, 512], P(('ep', 'tp')), may hold values from -6 to 6
- cache_rope: bfloat16 [128, 32, 512], P(('ep', 'tp')), may hold values from -6 to 6
- lengths: int32 [128], P('ep'), may hold values from 1 to 512, as said below
- moe_gain: float32 [1024], replicated, may hold values from 0.1 to 1.9
- route: int32 [128, 6], P('ep'), may hold values from 0 to 7, as said below
- route_weight: float32 [128, 6], P('ep'), may hold values from 0.1 to 1
- expert_gate: bfloat16 [8, 1024, 512], P('ep', None, 'tp'), may hold values from -0.1875 to 0.1875
- expert_up: bfloat16 [8, 1024, 512], P('ep', None, 'tp'), may hold values from -0.1875 to 0.1875
- expert_down: bfloat16 [8, 512, 1024], P('ep', 'tp'), may hold values from -0.25 to 0.25
Outputs:
- mixed_out: bfloat16 [128, 1024], P('ep', 'tp')
- new_latent: bfloat16 [128, 512], P('ep', 'tp')
- new_rope: bfloat16 [128, 32], P('ep')
Inputs may be any that keep to these rules, and one draw needn't show every extreme that they name: `route`: each row names 6 different experts that lie in one group of 8 consecutive expert numbers. Among the rows of the 16 sequences of one index of ep no expert is named more than 12 times, and some expert is named exactly 12 times by the rows of every index of ep. `lengths`: some sequence has exactly 512 cached positions.
All inputs are finite; a program needn't handle non-finite values.
Results may differ from a plain program's by a relative error of at most 0.02.
Values may be sent and summed in bfloat16 or wider, within the bound.
A program may use at most 64 MiB of HBM per device.

v0:
```python
import jax
import jax.numpy as jnp
from jax import lax
from jax.sharding import PartitionSpec as P

NOPE = 64
VDIM = 64
QK = 96
EPG = 8


EPS = 1e-06
ROPE_BASE = 10000.0


def rms_scaled(values_in, gain_vec):
    values_in = values_in.astype(jnp.float32)
    return (
        values_in
        * lax.rsqrt(jnp.mean(values_in * values_in, axis=-1, keepdims=True) + EPS)
        * gain_vec
    )


def rotate_last(values_in, positions):
    half_dim = values_in.shape[-1] // 2
    inverse = ROPE_BASE ** (-jnp.arange(half_dim, dtype=jnp.float32) / half_dim)
    angles = positions.astype(jnp.float32)[..., None] * inverse
    lower_half = values_in[..., :half_dim]
    upper_half = values_in[..., half_dim:]
    return jnp.concatenate(
        [
            lower_half * jnp.cos(angles) - upper_half * jnp.sin(angles),
            upper_half * jnp.cos(angles) + lower_half * jnp.sin(angles),
        ],
        -1,
    )


def rotate_rows(values_in, positions):
    half_dim = values_in.shape[1] // 2
    inverse = ROPE_BASE ** (-jnp.arange(half_dim, dtype=jnp.float32) / half_dim)
    angles = inverse[:, None] * positions.astype(jnp.float32)[None, :]
    lower_half = values_in[:, :half_dim]
    upper_half = values_in[:, half_dim:]
    return jnp.concatenate(
        [
            lower_half * jnp.cos(angles) - upper_half * jnp.sin(angles),
            upper_half * jnp.cos(angles) + lower_half * jnp.sin(angles),
        ],
        1,
    )


def shards(
    tokens,
    attn_gain,
    q_down,
    kv_down,
    rope_down,
    q_latent_gain,
    kv_latent_gain,
    q_up,
    query_gain,
    key_up,
    value_up,
    attn_out,
    cache_latent,
    cache_rope,
    lengths,
    moe_gain,
    route,
    route_weight,
    expert_gate,
    expert_up,
    expert_down,
):
    score_scale = QK ** (-0.5)
    tp_count = lax.axis_size("tp")
    tp_index = lax.axis_index("tp")
    normed = rms_scaled(tokens, attn_gain).astype(jnp.bfloat16)
    q_part = jnp.dot(normed, q_down, preferred_element_type=jnp.float32).astype(jnp.bfloat16)
    kv_part = jnp.dot(normed, kv_down, preferred_element_type=jnp.float32).astype(jnp.bfloat16)
    q_raw, kv_raw = (
        lax.all_gather(q_part, "tp", axis=1, tiled=True),
        lax.all_gather(kv_part, "tp", axis=1, tiled=True),
    )
    new_rope = jnp.dot(normed, rope_down, preferred_element_type=jnp.float32).astype(jnp.bfloat16)
    q_lat = rms_scaled(q_raw, q_latent_gain).astype(jnp.bfloat16)
    latent_new = rms_scaled(kv_raw, kv_latent_gain).astype(jnp.bfloat16)
    kv_cols = kv_part.shape[1]
    new_latent = lax.dynamic_slice_in_dim(latent_new, tp_index * kv_cols, kv_cols, 1)
    heads_here = query_gain.shape[0]
    seq_count = tokens.shape[0]
    query_head = rms_scaled(
        jnp.dot(q_lat, q_up, preferred_element_type=jnp.float32).reshape(seq_count, heads_here, QK),
        query_gain,
    )
    query_head = jnp.concatenate(
        [query_head[..., :NOPE], rotate_last(query_head[..., NOPE:], lengths[:, None])], -1
    ).astype(jnp.bfloat16)
    absorbed = jnp.einsum(
        "shn,rhn->shr",
        query_head[..., :NOPE],
        key_up.reshape(-1, heads_here, NOPE),
        preferred_element_type=jnp.float32,
    ).astype(jnp.bfloat16)
    rot_query = query_head[..., NOPE:]
    absorbed_mine, rot_mine = (
        lax.all_to_all(absorbed, "tp", split_axis=0, concat_axis=1, tiled=True),
        lax.all_to_all(rot_query, "tp", split_axis=0, concat_axis=1, tiled=True),
    )
    seqs_mine = cache_latent.shape[0]
    first_seq = tp_index * seqs_mine
    len_mine = lax.dynamic_slice_in_dim(lengths, first_seq, seqs_mine, 0)
    latent_mine = lax.dynamic_slice_in_dim(latent_new, first_seq, seqs_mine, 0)
    key_new = rotate_last(
        lax.dynamic_slice_in_dim(new_rope, first_seq, seqs_mine, 0).astype(jnp.float32), len_mine
    ).astype(jnp.bfloat16)
    positions = jnp.arange(cache_latent.shape[1], dtype=jnp.int32)
    rotated_keys = rotate_rows(cache_rope.astype(jnp.float32), positions).astype(jnp.bfloat16)
    scores = (
        jnp.einsum("shr,sjr->shj", absorbed_mine, cache_latent, preferred_element_type=jnp.float32)
        + jnp.einsum("shp,spj->shj", rot_mine, rotated_keys, preferred_element_type=jnp.float32)
    ) * score_scale
    self_score = (
        jnp.einsum("shr,sr->sh", absorbed_mine, latent_mine, preferred_element_type=jnp.float32)
        + jnp.einsum("shp,sp->sh", rot_mine, key_new, preferred_element_type=jnp.float32)
    ) * score_scale
    valid_keys = positions[None, :] < len_mine[:, None]
    masked = jnp.where(valid_keys[:, None, :], scores, -jnp.inf)
    row_max = jnp.maximum(jnp.max(masked, axis=-1), self_score)
    weights = jnp.exp(masked - row_max[..., None])
    self_weight = jnp.exp(self_score - row_max)
    total_weight = jnp.sum(weights, axis=-1) + self_weight
    latent_sum = jnp.einsum(
        "shj,sjr->shr",
        weights.astype(jnp.bfloat16),
        cache_latent,
        preferred_element_type=jnp.float32,
    )
    latent_sum = (
        latent_sum
        + self_weight.astype(jnp.bfloat16).astype(jnp.float32)[..., None]
        * latent_mine.astype(jnp.float32)[:, None, :]
    )
    attended = (latent_sum / total_weight[..., None]).astype(jnp.bfloat16)
    attended_heads = lax.all_to_all(attended, "tp", split_axis=1, concat_axis=0, tiled=True)
    head_values = (
        jnp.einsum(
            "shr,rhv->shv",
            attended_heads,
            value_up.reshape(-1, heads_here, VDIM),
            preferred_element_type=jnp.float32,
        )
        .astype(jnp.bfloat16)
        .reshape(seq_count, heads_here * VDIM)
    )
    head_sum = lax.psum(
        jnp.dot(head_values, attn_out, preferred_element_type=jnp.float32).astype(jnp.bfloat16),
        "tp",
    ).astype(jnp.float32)
    attn_resid = (tokens.astype(jnp.float32) + head_sum).astype(jnp.bfloat16)
    moe_input = rms_scaled(attn_resid, moe_gain).astype(jnp.bfloat16)
    topk_here = route.shape[1]
    experts_all = expert_gate.shape[0] * lax.axis_size("ep")
    group_cap = min(seq_count, max(2, 2 * seq_count * EPG // experts_all))
    capacity = (topk_here * group_cap + EPG - 1) // EPG
    flat_route = route.reshape(-1)
    row_order = jnp.arange(flat_route.shape[0])
    slot_rank = jnp.sum(
        (flat_route[:, None] == flat_route[None, :]) & (row_order[None, :] < row_order[:, None]),
        axis=1,
    )
    slot_index = flat_route * capacity + slot_rank
    model_width = tokens.shape[1]
    quarter_cols = model_width // tp_count
    residual = lax.dynamic_slice_in_dim(attn_resid, tp_index * quarter_cols, quarter_cols, 1)
    own_cols = lax.dynamic_slice_in_dim(moe_input, tp_index * quarter_cols, quarter_cols, 1)
    buffer = jnp.zeros((experts_all * capacity, own_cols.shape[1]), jnp.bfloat16)
    buffer = buffer.at[slot_index].set(jnp.repeat(own_cols, topk_here, axis=0))
    arrived = lax.all_to_all(
        buffer.reshape(experts_all, capacity, own_cols.shape[1]),
        "ep",
        split_axis=0,
        concat_axis=1,
        tiled=True,
    )
    piece = lax.all_gather(arrived, "tp", axis=2, tiled=True)
    gate_pre = jnp.einsum("erd,edf->erf", piece, expert_gate, preferred_element_type=jnp.float32)
    up_pre = jnp.einsum("erd,edf->erf", piece, expert_up, preferred_element_type=jnp.float32)
    hidden = (jax.nn.silu(gate_pre) * up_pre).astype(jnp.bfloat16)
    partial_value = jnp.einsum(
        "erf,efd->erd", hidden, expert_down, preferred_element_type=jnp.float32
    )
    reduced = lax.psum_scatter(
        partial_value.astype(jnp.bfloat16), "tp", scatter_dimension=2, tiled=True
    )
    returned = lax.all_to_all(reduced, "ep", split_axis=1, concat_axis=0, tiled=True)
    picked = (
        returned.reshape(-1, quarter_cols)[slot_index]
        .astype(jnp.float32)
        .reshape(seq_count, topk_here, quarter_cols)
    )
    mixed_out = (
        residual.astype(jnp.float32) + jnp.sum(picked * route_weight[..., None], axis=1)
    ).astype(jnp.bfloat16)
    return (mixed_out, new_latent, new_rope)


def solution(mesh):
    placed = (
        P("ep", None),
        P(),
        P(None, "tp"),
        P(None, "tp"),
        P(),
        P(),
        P(),
        P(None, "tp"),
        P("tp", None),
        P(None, "tp"),
        P(None, "tp"),
        P("tp", None),
        P(("ep", "tp"), None, None),
        P(("ep", "tp"), None, None),
        P("ep"),
        P(),
        P("ep", None),
        P("ep", None),
        P("ep", None, "tp"),
        P("ep", None, "tp"),
        P("ep", "tp", None),
    )
    return jax.shard_map(
        shards,
        mesh=mesh,
        in_specs=placed,
        out_specs=(P("ep", "tp"), P("ep", "tp"), P("ep", None)),
        check_vma=False,
    )
```

profile of v0, /device:TPU:0, one launch (start us, length us, event | category | flops | bytes accessed | tf_op | source)
XLA Modules:
  0.0 125.3 jit_solution(8537989430489213607)
XLA Ops:
  7.2 1.0 fusion.19
  8.3 1.2 convolution_convert_fusion.6
  9.5 6.1 %all_gather.9 = bf16[16,512]{1,0:T(8,128)(2,1)S(1)} all-gather(bf16[16,128]{1,0:T(8,128)(2,1)S(1)} %convolution_convert_fusion.6), channel_id=1, replica_groups=mesh['ep'=8,'tp'=4] {'tp'}, dimensions={1}, use_global_device_ids=true | all-gather | bytes 20480 | tf_op jit(solution)/shard_map/all_gather | solution.py:85
  15.7 1.1 fusion.42
  19.5 3.3 %all-to-all-start.1 = ((bf16[4,2,128]{2,1,0:T(2,128)(2,1)}), bf16[4,2,128]{2,1,0:T(2,128)(2,1)S(1)}, u32[]{:S(2)}, u32[]{:S(2)}) async-start(bf16[4,2,128]{2,1,0:T(2,128)(2,1)} %reshape.330), calls=%async_computation.1 | async-start | bytes 4096 | tf_op jit(solution)/shard_map/all_to_all | solution.py:111
  24.5 1.0 copy.90
  25.7 0.9 convert_element_type.133
  27.6 1.2 convolution_convert_fusion.5
  28.8 5.4 %all_gather.10 = bf16[16,512]{1,0:T(8,128)(2,1)S(1)} all-gather(bf16[16,128]{1,0:T(8,128)(2,1)S(1)} %convolution_convert_fusion.5), channel_id=1, replica_groups=mesh['ep'=8,'tp'=4] {'tp'}, dimensions={1}, use_global_device_ids=true | all-gather | bytes 20480 | tf_op jit(solution)/shard_map/all_gather | solution.py:86
  35.7 3.3 %all-to-all-start = ((bf16[16,2,512]{2,1,0:T(2,128)(2,1)}), bf16[16,2,512]{2,1,0:T(2,128)(2,1)S(1)}, u32[]{:S(2)}, u32[]{:S(2)}) async-start(bf16[16,2,512]{2,1,0:T(2,128)(2,1)} %copy.91), calls=%async_computation | async-start | bytes 65536 | tf_op jit(solution)/shard_map/all_to_all | solution.py:110
  39.2 3.7 %all-to-all-done = bf16[16,2,512]{2,1,0:T(2,128)(2,1)S(1)} async-done(((bf16[16,2,512]{2,1,0:T(2,128)(2,1)}), bf16[16,2,512]{2,1,0:T(2,128)(2,1)S(1)}, u32[]{:S(2)}, u32[]{:S(2)}) %all-to-all-start) | async-done | bytes 32800 | tf_op jit(solution)/shard_map/all_to_all | solution.py:110
  45.3 3.3 %all-to-all-start.2 = ((bf16[4,8,512]{2,0,1:T(4,128)(2,1)}), bf16[4,8,512]{2,0,1:T(4,128)(2,1)S(1)}, u32[]{:S(2)}, u32[]{:S(2)}) async-start(bf16[4,8,512]{2,0,1:T(4,128)(2,1)} %copy.95), calls=%async_computation.2 | async-start | bytes 65536 | tf_op jit(solution)/shard_map/all_to_all | solution.py:148
  49.5 2.9 %all-to-all-done.2 = bf16[4,8,512]{2,0,1:T(4,128)(2,1)S(1)} async-done(((bf16[4,8,512]{2,0,1:T(4,128)(2,1)}), bf16[4,8,512]{2,0,1:T(4,128)(2,1)S(1)}, u32[]{:S(2)}, u32[]{:S(2)}) %all-to-all-start.2) | async-done | bytes 32800 | tf_op jit(solution)/shard_map/all_to_all | solution.py:148
  52.9 10.3 %psum.7 = bf16[16,1024]{1,0:T(8,128)(2,1)S(1)} all-reduce(bf16[16,1024]{1,0:T(8,128)(2,1)S(1)} %convolution_convert_fusion.1), channel_id=1, replica_groups=mesh['ep'=8,'tp'=4] {'tp'}, use_global_device_ids=true, to_apply=%region_6.7 | all-reduce | flops 16384 | bytes 65536 | tf_op jit(solution)/shard_map/psum | solution.py:159
  63.4 0.9 scatter_custom_fusion
  64.4 12.8 %all_to_all.75 = bf16[8,12,256]{2,1,0:T(8,128)(2,1)S(1)} all-to-all(bf16[8,12,256]{2,1,0:T(8,128)(2,1)S(1)} %reshape.301), channel_id=1, replica_groups=mesh['ep'=8,'tp'=4] {'ep'}, dimensions={0} | all-to-all | bytes 98304 | tf_op jit(solution)/shard_map/all_to_all | solution.py:182
  77.2 5.6 %all_gather.11 = bf16[1,96,1024]{2,1,0:T(8,128)(2,1)S(1)} all-gather(bf16[1,96,256]{2,1,0:T(8,128)(2,1)S(1)} %all_to_all.68), channel_id=1, replica_groups=mesh['ep'=8,'tp'=4] {'tp'}, dimensions={2}, use_global_device_ids=true | all-gather | bytes 245760 | tf_op jit(solution)/shard_map/all_gather | solution.py:189
  83.1 1.0 fusion
  84.2 17.4 %reduce-scatter.2.cloned.1.call-done = bf16[1,96,256]{2,1,0:T(8,128)(2,1)} async-done(((bf16[1,96,1024]{2,1,0:T(8,128)(2,1)}), bf16[1,96,256]{2,1,0:T(8,128)(2,1)}) %reduce-scatter.2.cloned.1.call-update) | async-done | bytes 49168 | tf_op jit(solution)/shard_map/reduce_scatter | solution.py:196
  101.6 0.9 copy.122
  103.0 0.9 reduce
  104.6 5.5 %all-to-all-start.4 = ((bf16[8,2,1536]{2,1,0:T(2,128)(2,1)}), bf16[8,2,1536]{2,1,0:T(2,128)(2,1)S(1)}, u32[]{:S(2)}, u32[]{:S(2)}) async-start(bf16[8,2,1536]{2,1,0:T(2,128)(2,1)} %reshape.332), calls=%async_computation.5 | async-start | bytes 98304 | tf_op jit(solution)/shard_map/all_to_all | solution.py:199
  110.7 6.2 %all-to-all-done.4 = bf16[8,2,1536]{2,1,0:T(2,128)(2,1)S(1)} async-done(((bf16[8,2,1536]{2,1,0:T(2,128)(2,1)}), bf16[8,2,1536]{2,1,0:T(2,128)(2,1)S(1)}, u32[]{:S(2)}, u32[]{:S(2)}) %all-to-all-start.4) | async-done | bytes 49184 | tf_op jit(solution)/shard_map/all_to_all | solution.py:199
  116.9 0.8 gather_fusion
  (104 shorter events, 14.1 us)
Async XLA Ops:
  7.2 35.8 %copy-start = (bf16[4,512,512]{2,1,0:T(8,128)(2,1)S(1)}, bf16[4,512,512]{2,1,0:T(8,128)(2,1)}, u32[]{:S(2)}) copy-start(bf16[4,512,512]{2,1,0:T(8,128)(2,1)} %param.33) | copy-start | bytes 6291460
  7.2 27.3 %copy-start.5 = (bf16[16,1024]{1,0:T(8,128)(2,1)S(1)}, bf16[16,1024]{1,0:T(8,128)(2,1)}, u32[]{:S(2)}) copy-start(bf16[16,1024]{1,0:T(8,128)(2,1)} %param.21) | copy-start | bytes 98308
  7.2 27.3 %copy-start.11 = (f32[1024]{0:T(1024)S(1)}, f32[1024]{0:T(1024)}, u32[]{:S(2)}) copy-start(f32[1024]{0:T(1024)} %param.22) | copy-start | bytes 12292
  7.2 27.1 %copy-start.8 = (f32[512]{0:T(512)S(1)}, f32[512]{0:T(512)}, u32[]{:S(2)}) copy-start(f32[512]{0:T(512)} %param.27) | copy-start | bytes 6148
  7.2 27.2 %copy-start.10 = (bf16[1024,32]{0,1:T(8,128)(2,1)S(1)}, bf16[1024,32]{0,1:T(8,128)(2,1)}, u32[]{:S(2)}) copy-start(bf16[1024,32]{0,1:T(8,128)(2,1)} %param.25) | copy-start | bytes 196612
  19.5 16.2 %all-to-all-start.1 = ((bf16[4,2,128]{2,1,0:T(2,128)(2,1)}), bf16[4,2,128]{2,1,0:T(2,128)(2,1)S(1)}, u32[]{:S(2)}, u32[]{:S(2)}) async-start(bf16[4,2,128]{2,1,0:T(2,128)(2,1)} %reshape.330), calls=%async_computation.1 | async-start | bytes 4096 | tf_op jit(solution)/shard_map/all_to_all | solution.py:111
  34.7 10.0 %copy-start.9 = (bf16[16,32]{1,0:T(8,128)(2,1)}, bf16[16,32]{1,0:T(8,128)(2,1)S(1)}, u32[]{:S(2)}) copy-start(bf16[16,32]{1,0:T(8,128)(2,1)S(1)} %convolution_convert_fusion.4) | copy-start | bytes 3076
  35.7 7.2 %all-to-all-start = ((bf16[16,2,512]{2,1,0:T(2,128)(2,1)}), bf16[16,2,512]{2,1,0:T(2,128)(2,1)S(1)}, u32[]{:S(2)}, u32[]{:S(2)}) async-start(bf16[16,2,512]{2,1,0:T(2,128)(2,1)} %copy.91), calls=%async_computation | async-start | bytes 65536 | tf_op jit(solution)/shard_map/all_to_all | solution.py:110
  43.0 5.6 %copy-start.6 = (bf16[512,128]{1,0:T(8,128)(2,1)S(1)}, bf16[512,128]{1,0:T(8,128)(2,1)}, u32[]{:S(2)}) copy-start(bf16[512,128]{1,0:T(8,128)(2,1)} %param.31) | copy-start | bytes 393220
  43.6 9.1 %copy-start.1 = (bf16[128,1024]{1,0:T(8,128)(2,1)S(1)}, bf16[128,1024]{1,0:T(8,128)(2,1)}, u32[]{:S(2)}) copy-start(bf16[128,1024]{1,0:T(8,128)(2,1)} %param.32) | copy-start | bytes 786436
  44.2 38.6 %copy-start.2 = (bf16[1,1024,128]{2,1,0:T(8,128)(2,1)S(1)}, bf16[1,1024,128]{2,1,0:T(8,128)(2,1)}, u32[]{:S(2)}) copy-start(bf16[1,1024,128]{2,1,0:T(8,128)(2,1)} %param.39) | copy-start | bytes 786436
  44.2 38.8 %copy-start.3 = (bf16[1,128,1024]{2,1,0:T(8,128)(2,1)S(1)}, bf16[1,128,1024]{2,1,0:T(8,128)(2,1)}, u32[]{:S(2)}) copy-start(bf16[1,128,1024]{2,1,0:T(8,128)(2,1)} %param.41) | copy-start | bytes 786436
  44.2 38.8 %copy-start.4 = (bf16[1,1024,128]{2,1,0:T(8,128)(2,1)S(1)}, bf16[1,1024,128]{2,1,0:T(8,128)(2,1)}, u32[]{:S(2)}) copy-start(bf16[1,1024,128]{2,1,0:T(8,128)(2,1)} %param.40) | copy-start | bytes 786436
  44.7 39.5 %copy-start.7 = (f32[16,6]{0,1:T(8,128)S(1)}, f32[16,6]{0,1:T(8,128)}, u32[]{:S(2)}) copy-start(f32[16,6]{0,1:T(8,128)} %param.38) | copy-start | bytes 1156
  45.3 7.2 %all-to-all-start.2 = ((bf16[4,8,512]{2,0,1:T(4,128)(2,1)}), bf16[4,8,512]{2,0,1:T(4,128)(2,1)S(1)}, u32[]{:S(2)}, u32[]{:S(2)}) async-start(bf16[4,8,512]{2,0,1:T(4,128)(2,1)} %copy.95), calls=%async_computation.2 | async-start | bytes 65536 | tf_op jit(solution)/shard_map/all_to_all | solution.py:148
  48.6 53.1 %reduce-scatter.2.cloned.1.call-start = ((), (), s32[]{:S(2)}) async-start(), calls=%async_computation.6 | async-start | bytes 245760 | tf_op jit(solution)/shard_map/reduce_scatter | solution.py:196
  104.6 12.3 %all-to-all-start.4 = ((bf16[8,2,1536]{2,1,0:T(2,128)(2,1)}), bf16[8,2,1536]{2,1,0:T(2,128)(2,1)S(1)}, u32[]{:S(2)}, u32[]{:S(2)}) async-start(bf16[8,2,1536]{2,1,0:T(2,128)(2,1)} %reshape.332), calls=%async_computation.5 | async-start | bytes 98304 | tf_op jit(solution)/shard_map/all_to_all | solution.py:199
Sparse Core Ops, SparseCore 0:
  84.2 17.3 reduce-scatter.1
where the time goes:
time: 126 us; the launch traced here: 125 us
  blocking collectives  40.2 us (32%)
  waiting for transfers between devices  30.3 us (24%)
  starting transfers between devices  15.3 us (12%)
  between operations  14.4 us (11%)
  local copies, waits for them, and re-layouts  9.87 us (8%)
  other arithmetic  8.27 us (7%)
  matrix products  6.88 us (5%)
    reduce_scatter x1, waiting for transfers between devices, shards(): lax.psum_scatter(partial_value.astype(jnp.bfloat16), 'tp', scatter_dimens...  17.4 us
    all_to_all x1, blocking collectives, shards(): lax.all_to_all(buffer.reshape(experts_all, capacity, own_cols.shape[1]),...  12.8 us
    psum x1, blocking collectives, shards(): lax.psum(jnp.dot(head_values, attn_out, preferred_element_type=jnp.float3...  10.3 us
    all_to_all x1, waiting for transfers between devices, shards(): lax.all_to_all(reduced, 'ep', split_axis=1, concat_axis=0, tiled=True)  6.2 us
    all_gather x1, blocking collectives, shards(): lax.all_gather(q_part, 'tp', axis=1, tiled=True)  6.14 us
    all_gather x1, blocking collectives, shards(): piece = lax.all_gather(arrived, 'tp', axis=2, tiled=True)  5.6 us
    all_to_all x1, starting transfers between devices, shards(): lax.all_to_all(reduced, 'ep', split_axis=1, concat_axis=0, tiled=True)  5.52 us
    all_gather x1, blocking collectives, shards(): lax.all_gather(kv_part, 'tp', axis=1, tiled=True)  5.42 us
  transfers between devices with their start and end apart: 5, of which 4 were waited for; matrix products, arithmetic and copies ran while one was open for 7% of the time, Pallas kernels for 0%

commit v1 on v0

v1 whole, which is shorter than its diff:
```python
import functools
import math

import jax
import jax.numpy as jnp
from jax import lax
from jax.experimental import pallas as pl
from jax.experimental.pallas import tpu as pltpu
from jax.sharding import PartitionSpec as P

NOPE = 64
EPS = 1e-06
ROPE_BASE = 10000.0
MESH = pl.DeviceIdType.MESH
BF = jnp.bfloat16
F32 = jnp.float32


def shift_of(n):
    s = n.bit_length() - 1
    assert 1 << s == n
    return s


def div(v, n):
    return lax.shift_right_logical(v, jnp.int32(shift_of(n)))


def mod(v, n):
    return jnp.bitwise_and(v, jnp.int32(n - 1))


def iota(shape, dim):
    return lax.broadcasted_iota(jnp.int32, shape, dim)


def mm(a, b):
    return jnp.dot(a, b, preferred_element_type=F32)


def mm_nt(a, b):
    return lax.dot_general(a, b, (((1,), (1,)), ((), ())), preferred_element_type=F32)


def exact(a, b):
    return jnp.dot(a, b, preferred_element_type=F32, precision=lax.Precision.HIGHEST)


def kernel(
    ep_n,
    tp_n,
    tokens,
    attn_gain,
    q_down_h,
    kv_down_h,
    rope_down_h,
    q_gain,
    kv_gain,
    q_up_h,
    query_gain,
    key_up_h,
    value_up_h,
    attn_out_h,
    cache_h,
    rope_h,
    lengths,
    moe_gain,
    route,
    route_weight,
    gate_h,
    up_h,
    down_h,
    mixed_ref,
    latent_ref,
    rope_ref,
    q_down,
    kv_down,
    rope_down,
    q_up,
    key_up,
    value_up,
    attn_out,
    cache,
    crope,
    gate_w,
    up_w,
    down_w,
    lat_buf,
    query_out,
    query_in,
    att_out,
    att_in,
    sum_out,
    sum_in,
    rows_in,
    part_out,
    part_in,
    load_sem,
    tp_send,
    tp_recv,
    all_send,
    all_recv,
):
    ep_me = lax.axis_index("ep")
    me = lax.axis_index("tp")
    n = ep_n * tp_n
    lin = ep_me * tp_n + me
    seqs = tokens.shape[0]
    cols = tokens.shape[1] // tp_n
    heads, qk = query_gain.shape
    ropes = qk - NOPE
    half = ropes // 2
    s_here = cache.shape[0]
    rank = cache.shape[2]
    rows = tp_n * heads * s_here
    block = heads * s_here
    lanes = 128

    loads = [
        pltpu.make_async_copy(src, dst, load_sem.at[i])
        for i, (src, dst) in enumerate(
            [
                (q_down_h, q_down),
                (kv_down_h, kv_down),
                (rope_down_h, rope_down),
                (q_up_h, q_up),
                (key_up_h, key_up),
                (rope_h, crope),
                (cache_h, cache),
                (value_up_h, value_up),
                (attn_out_h, attn_out),
                (gate_h, gate_w),
                (up_h, up_w),
                (down_h, down_w),
            ]
        )
    ]
    for load in loads:
        load.start()

    barrier = pltpu.get_barrier_semaphore()

    def greet(k, carry):
        to = lax.rem(lin + k, n)
        pl.semaphore_signal(barrier, inc=1, device_id=(to // tp_n, lax.rem(to, tp_n)), device_id_type=MESH)
        return carry

    lax.fori_loop(1, n, greet, 0)

    def tp_copy(stage, src, dst, to, origin):
        return pltpu.make_async_remote_copy(
            src_ref=src,
            dst_ref=dst,
            send_sem=tp_send.at[stage, to],
            recv_sem=tp_recv.at[stage, origin],
            device_id=(ep_me, to),
            device_id_type=MESH,
        )

    def exchange(stage, src_of, dst_of):
        for k in range(1, tp_n):
            to = lax.rem(me + k, tp_n)
            tp_copy(stage, src_of(to), dst_of(me), to, me).start()

    def arrive(stage, src_of, dst_of):
        for k in range(1, tp_n):
            other = lax.rem(me + k, tp_n)
            tp_copy(stage, src_of(other), dst_of(other), other, other).wait_recv()

    def sent(stage, src_of, dst_of):
        for k in range(1, tp_n):
            other = lax.rem(me + k, tp_n)
            tp_copy(stage, src_of(other), dst_of(other), other, other).wait_send()

    tok = tokens[...].astype(F32)
    normed = (tok * lax.rsqrt(jnp.mean(tok * tok, axis=-1, keepdims=True) + EPS) * attn_gain[...]).astype(BF)
    loads[0].wait()
    qc = q_down.shape[1]
    kc = kv_down.shape[1]
    q_part = mm(normed, q_down[...]).astype(BF)
    loads[1].wait()
    kv_part = mm(normed, kv_down[...]).astype(BF)
    lat_buf[me, :, :qc] = q_part
    lat_buf[me, :, qc:] = kv_part
    pl.semaphore_wait(barrier, n - 1)
    own_lat = lambda to: lat_buf.at[me]
    lat_at = lambda i: lat_buf.at[i]
    exchange(0, own_lat, lat_at)

    loads[2].wait()
    new_rope = mm(normed, rope_down[...]).astype(BF)
    rope_ref[...] = new_rope
    len_row = lengths[...].astype(F32)
    eye = iota((seqs, seqs), 0) == iota((seqs, seqs), 1)
    len_col = jnp.sum(jnp.where(eye, len_row, 0.0), axis=1, keepdims=True)
    lane1 = iota((1, lanes), 1)
    inv_lane = jnp.exp(mod(lane1, half).astype(F32) * (-math.log(ROPE_BASE) / half))
    ang = len_col * inv_lane
    cos_q, sin_q = jnp.cos(ang), jnp.sin(ang)

    width = heads * qk
    src_i, out_c = iota((width, lanes), 0), iota((width, lanes), 1)
    pick_n = jnp.where(src_i == div(out_c, NOPE) * qk + mod(out_c, NOPE), 1.0, 0.0).astype(BF)
    rope_head, rope_p = div(out_c, ropes), mod(out_c, ropes)
    live = out_c < heads * ropes
    pick_a = jnp.where(live & (src_i == rope_head * qk + NOPE + rope_p), 1.0, 0.0)
    pick_b = jnp.where(
        live & (src_i == rope_head * qk + NOPE + mod(rope_p + half, ropes)),
        jnp.where(rope_p < half, -1.0, 1.0),
        0.0,
    )
    key_i, key_c = iota((ropes, lanes), 0), iota((ropes, lanes), 1)
    key_p = mod(key_c, ropes)
    key_a = jnp.where(key_i == key_p, 1.0, 0.0).astype(BF)
    key_b = jnp.where(key_i == mod(key_p + half, ropes), jnp.where(key_p < half, -1.0, 1.0), 0.0).astype(BF)
    key_new = (mm(new_rope, key_a) * cos_q + mm(new_rope, key_b) * sin_q).astype(BF)

    g_i, g_c = iota((qk, width), 0), iota((qk, width), 1)
    tile = jnp.zeros((qk, width), F32)
    for h in range(heads):
        tile = jnp.where(g_c - h * qk == g_i, 1.0, tile)
    gains = exact(query_gain[...], tile)
    lane_w = iota((1, width), 1)
    gain = gains[0:1]
    for h in range(1, heads):
        gain = jnp.where(lane_w >= h * qk, gains[h : h + 1], gain)

    row_i, seq_c = iota((rows, seqs), 0), iota((rows, seqs), 1)
    spread = jnp.where(div(row_i, block) * s_here + mod(row_i, s_here) == seq_c, 1.0, 0.0).astype(BF)
    mine_mask = me * s_here + mod(row_i, s_here) == seq_c
    mine = jnp.where(mine_mask, 1.0, 0.0).astype(BF)
    len_rows = jnp.sum(jnp.where(mine_mask, len_row, 0.0), axis=1, keepdims=True)
    row_l, lane_l = iota((rows, lanes), 0), iota((rows, lanes), 1)
    row_head = mod(div(row_l, s_here), heads)
    head_lanes = div(lane_l, NOPE) == row_head
    rope_lanes = div(lane_l, ropes) == row_head

    loads[5].wait()
    positions = crope.shape[2]
    inv_sub = jnp.exp(iota((half, positions), 0).astype(F32) * (-math.log(ROPE_BASE) / half))
    kang = inv_sub * iota((half, positions), 1).astype(F32)
    kcos, ksin = jnp.cos(kang), jnp.sin(kang)
    rotated = []
    pad = jnp.zeros((lanes - heads * ropes, positions), BF)
    for s in range(s_here):
        u = crope[s, :half, :].astype(F32)
        w = crope[s, half:, :].astype(F32)
        a = (u * kcos - w * ksin).astype(BF)
        b = (w * kcos + u * ksin).astype(BF)
        rotated.append(jnp.concatenate([a, b] * heads + [pad], axis=0))

    arrive(0, own_lat, lat_at)
    q_raw = jnp.concatenate([lat_buf[t, :, :qc] for t in range(tp_n)], axis=1).astype(F32)
    kv_raw = jnp.concatenate([lat_buf[t, :, qc:] for t in range(tp_n)], axis=1).astype(F32)
    q_lat = (q_raw * lax.rsqrt(jnp.mean(q_raw * q_raw, axis=-1, keepdims=True) + EPS) * q_gain[...]).astype(BF)
    loads[3].wait()
    query = mm(q_lat, q_up[...])
    scale = jnp.zeros_like(query)
    lane_q = iota(query.shape, 1)
    for h in range(heads):
        inside = (lane_q >= h * qk) & (lane_q < (h + 1) * qk)
        total = jnp.sum(jnp.where(inside, query * query, 0.0), axis=-1, keepdims=True)
        scale = jnp.where(inside, lax.rsqrt(total * (1.0 / qk) + EPS), scale)
    query = query * scale * gain
    nope = mm(query.astype(BF), pick_n).astype(BF)
    rot = (exact(query, pick_a) * cos_q + exact(query, pick_b) * sin_q).astype(BF)
    nope_rows = jnp.where(head_lanes, mm(spread, nope), 0.0).astype(BF)
    rot_rows = jnp.where(rope_lanes, mm(spread, rot), 0.0).astype(BF)
    loads[4].wait()
    absorbed = mm_nt(nope_rows, key_up[...]).astype(BF)
    for t in range(tp_n):
        query_out[t, :, :rank] = absorbed[t * block : (t + 1) * block]
        query_out[t, :, rank:] = rot_rows[t * block : (t + 1) * block]
    q_src = lambda to: query_out.at[to]
    q_dst = lambda i: query_in.at[i]
    exchange(1, q_src, q_dst)
    query_in[me] = query_out[me]

    kv_scale = lax.rsqrt(jnp.mean(kv_raw * kv_raw, axis=-1, keepdims=True) + EPS)
    latent_new = (kv_raw * kv_scale * kv_gain[...]).astype(BF)
    own_cols = pl.ds(pl.multiple_of(me * kc, kc), kc)
    latent_ref[...] = (kv_part.astype(F32) * kv_scale * kv_gain[:, own_cols]).astype(BF)
    latent_rows = mm(mine, latent_new)
    key_rows = mm(mine, key_new)
    loads[6].wait()

    arrive(1, q_src, q_dst)
    q_abs = jnp.concatenate([query_in[t, :, :rank] for t in range(tp_n)], axis=0)
    q_rot = jnp.concatenate([query_in[t, :, rank:] for t in range(tp_n)], axis=0)
    row_p, pos_p = iota((rows, positions), 0), iota((rows, positions), 1)
    row_seq = mod(row_p, s_here)
    scores = jnp.zeros((rows, positions), F32)
    for s in range(s_here):
        scores = jnp.where(row_seq == s, mm_nt(q_abs, cache[s]) + mm(q_rot, rotated[s]), scores)
    score_scale = qk ** (-0.5)
    scores = scores * score_scale
    self_score = (
        jnp.sum(q_abs.astype(F32) * latent_rows, axis=-1, keepdims=True)
        + jnp.sum(q_rot.astype(F32) * key_rows, axis=-1, keepdims=True)
    ) * score_scale
    valid = pos_p.astype(F32) < len_rows
    scores = jnp.where(valid, scores, -jnp.inf)
    top = jnp.maximum(jnp.max(scores, axis=-1, keepdims=True), self_score)
    weights = jnp.exp(scores - top)
    self_weight = jnp.exp(self_score - top)
    total = jnp.sum(weights, axis=-1, keepdims=True) + self_weight
    acc = self_weight.astype(BF).astype(F32) * latent_rows
    for s in range(s_here):
        acc = acc + mm(jnp.where(row_seq == s, weights, 0.0).astype(BF), cache[s])
    attended = (acc / total).astype(BF)
    for t in range(tp_n):
        att_out[t] = attended[t * block : (t + 1) * block]
    a_src = lambda to: att_out.at[to]
    a_dst = lambda i: att_in.at[i]
    exchange(2, a_src, a_dst)
    att_in[me] = att_out[me]
    loads[7].wait()
    loads[8].wait()
    seq_i, row_c = iota((seqs, rows), 0), iota((seqs, rows), 1)
    gather = jnp.where(div(row_c, block) * s_here + mod(row_c, s_here) == seq_i, 1.0, 0.0).astype(BF)

    arrive(2, a_src, a_dst)
    att = jnp.concatenate([att_in[t] for t in range(tp_n)], axis=0)
    values = jnp.where(head_lanes, mm(att, value_up[...]), 0.0).astype(BF)
    head_values = mm(gather, values).astype(BF)
    partial = mm(head_values, attn_out[...]).astype(BF)
    for t in range(tp_n):
        sum_out[t] = partial[:, t * cols : (t + 1) * cols]
    s_src = lambda to: sum_out.at[to]
    s_dst = lambda i: sum_in.at[i]
    exchange(3, s_src, s_dst)
    sum_in[me] = sum_out[me]
    model_cols = pl.ds(pl.multiple_of(me * cols, cols), cols)
    tok_mine = tokens[:, model_cols].astype(F32)
    loads[9].wait()
    loads[10].wait()
    loads[11].wait()

    arrive(3, s_src, s_dst)
    head_sum = sum_in[0].astype(F32)
    for t in range(1, tp_n):
        head_sum = head_sum + sum_in[t].astype(F32)
    resid = (tok_mine + head_sum).astype(BF)
    rows_in[lin] = resid

    def all_copy(stage, src, dst, to):
        return pltpu.make_async_remote_copy(
            src_ref=src,
            dst_ref=dst,
            send_sem=all_send.at[stage],
            recv_sem=all_recv.at[stage],
            device_id=(to // tp_n, lax.rem(to, tp_n)),
            device_id_type=MESH,
        )

    def give_rows(k, carry):
        to = lax.rem(lin + k, n)
        all_copy(0, rows_in.at[lin], rows_in.at[lin], to).start()
        return carry

    lax.fori_loop(1, n, give_rows, 0)

    def all_wait(stage, src, dst):
        others = pl.ds(0, n - 1)
        return all_copy(stage, src.at[others], dst.at[others], lax.rem(lin + 1, n))

    all_wait(0, rows_in, rows_in).wait_recv()

    group = math.gcd(ep_n, 8)

    def expert(g, carry):
        first = g * group
        parts = []
        square = jnp.zeros((group * seqs, 1), F32)
        for t in range(tp_n):
            x = jnp.concatenate([rows_in[(first + i) * tp_n + t] for i in range(group)], axis=0).astype(F32)
            square = square + jnp.sum(x * x, axis=-1, keepdims=True)
            parts.append(x)
        inverse = lax.rsqrt(square * (1.0 / (cols * tp_n)) + EPS)
        gate = jnp.zeros((group * seqs, gate_w.shape[2]), F32)
        up = jnp.zeros((group * seqs, gate_w.shape[2]), F32)
        for t in range(tp_n):
            here = slice(t * cols, (t + 1) * cols)
            x = (parts[t] * inverse * moe_gain[:, here]).astype(BF)
            gate = gate + mm(x, gate_w[0, here, :])
            up = up + mm(x, up_w[0, here, :])
        hidden = (gate / (1.0 + jnp.exp(-gate)) * up).astype(BF)
        for t in range(tp_n):
            here = slice(t * cols, (t + 1) * cols)
            part = mm(hidden, down_w[0, :, here]).astype(BF)
            for i in range(group):
                part_out[(first + i) * tp_n + t] = part[i * seqs : (i + 1) * seqs]
        return carry

    if ep_n == group:
        expert(0, 0)
    else:
        lax.fori_loop(0, ep_n // group, expert, 0)

    def give_parts(k, carry):
        to = lax.rem(lin + k, n)
        all_copy(1, part_out.at[to], part_in.at[lin], to).start()
        return carry

    lax.fori_loop(1, n, give_parts, 0)
    part_in[lin] = part_out[lin]
    chosen = route[...]
    chosen_weight = route_weight[...]
    all_wait(1, part_out, part_in).wait_recv()

    def combine(e, mixed):
        found = part_in[e * tp_n].astype(F32)
        for t in range(1, tp_n):
            found = found + part_in[e * tp_n + t].astype(F32)
        share = jnp.sum(jnp.where(chosen == e, chosen_weight, 0.0), axis=1, keepdims=True)
        return mixed + share * found.astype(BF).astype(F32)

    mixed = jnp.zeros((seqs, cols), F32)
    if ep_n <= 8:
        for e in range(ep_n):
            mixed = combine(e, mixed)
    else:
        mixed = lax.fori_loop(0, ep_n, combine, mixed)
    mixed_ref[...] = (resid.astype(F32) + mixed).astype(BF)

    sent(0, own_lat, lat_at)
    sent(1, q_src, q_dst)
    sent(2, a_src, a_dst)
    sent(3, s_src, s_dst)
    all_wait(0, rows_in, rows_in).wait_send()
    all_wait(1, part_out, part_in).wait_send()


def shards(ep_n, tp_n, *args):
    (
        tokens,
        attn_gain,
        q_down,
        kv_down,
        rope_down,
        q_latent_gain,
        kv_latent_gain,
        q_up,
        query_gain,
        key_up,
        value_up,
        attn_out,
        cache_latent,
        cache_rope,
        lengths,
        moe_gain,
        route,
        route_weight,
        expert_gate,
        expert_up,
        expert_down,
    ) = args
    assert expert_gate.shape[0] == 1
    row = lambda v: v.reshape(1, -1)
    operands = (
        tokens,
        row(attn_gain),
        q_down,
        kv_down,
        rope_down,
        row(q_latent_gain),
        row(kv_latent_gain),
        q_up,
        query_gain,
        key_up,
        value_up,
        attn_out,
        cache_latent,
        cache_rope,
        row(lengths),
        row(moe_gain),
        route,
        route_weight,
        expert_gate,
        expert_up,
        expert_down,
    )
    far = {2, 3, 4, 7, 9, 10, 11, 12, 13, 18, 19, 20}
    vmem = pl.BlockSpec(memory_space=pltpu.VMEM)
    anyspace = pl.BlockSpec(memory_space=pl.ANY)
    seqs, model = tokens.shape
    cols = model // tp_n
    n = ep_n * tp_n
    heads = query_gain.shape[0]
    s_here, _, rank = cache_latent.shape
    block = heads * s_here
    like = lambda v: pltpu.VMEM(v.shape, v.dtype)
    scratch = [
        like(q_down),
        like(kv_down),
        like(rope_down),
        like(q_up),
        like(key_up),
        like(value_up),
        like(attn_out),
        like(cache_latent),
        like(cache_rope),
        like(expert_gate),
        like(expert_up),
        like(expert_down),
        pltpu.VMEM((tp_n, seqs, q_down.shape[1] + kv_down.shape[1]), BF),
        pltpu.VMEM((tp_n, block, rank + 128), BF),
        pltpu.VMEM((tp_n, block, rank + 128), BF),
        pltpu.VMEM((tp_n, block, rank), BF),
        pltpu.VMEM((tp_n, block, rank), BF),
        pltpu.VMEM((tp_n, seqs, cols), BF),
        pltpu.VMEM((tp_n, seqs, cols), BF),
        pltpu.VMEM((n, seqs, cols), BF),
        pltpu.VMEM((n, seqs, cols), BF),
        pltpu.VMEM((n, seqs, cols), BF),
        pltpu.SemaphoreType.DMA((12,)),
        pltpu.SemaphoreType.DMA((4, tp_n)),
        pltpu.SemaphoreType.DMA((4, tp_n)),
        pltpu.SemaphoreType.DMA((2,)),
        pltpu.SemaphoreType.DMA((2,)),
    ]
    return pl.pallas_call(
        functools.partial(kernel, ep_n, tp_n),
        out_shape=(
            jax.ShapeDtypeStruct((seqs, cols), BF),
            jax.ShapeDtypeStruct((seqs, kv_down.shape[1]), BF),
            jax.ShapeDtypeStruct((seqs, rope_down.shape[1]), BF),
        ),
        in_specs=[anyspace if i in far else vmem for i in range(len(operands))],
        out_specs=(vmem, vmem, vmem),
        scratch_shapes=scratch,
        compiler_params=pltpu.CompilerParams(
            collective_id=0, has_side_effects=True, vmem_limit_bytes=60 * 1024 * 1024
        ),
    )(*operands)


def solution(mesh):
    placed = (
        P("ep", None),
        P(),
        P(None, "tp"),
        P(None, "tp"),
        P(),
        P(),
        P(),
        P(None, "tp"),
        P("tp", None),
        P(None, "tp"),
        P(None, "tp"),
        P("tp", None),
        P(("ep", "tp"), None, None),
        P(("ep", "tp"), None, None),
        P("ep"),
        P(),
        P("ep", None),
        P("ep", None),
        P("ep", None, "tp"),
        P("ep", None, "tp"),
        P("ep", "tp", None),
    )
    return jax.shard_map(
        functools.partial(shards, mesh.shape["ep"], mesh.shape["tp"]),
        mesh=mesh,
        in_specs=placed,
        out_specs=(P("ep", "tp"), P("ep", "tp"), P("ep", None)),
        check_vma=False,
    )
```

time: 126 us -> 47.1 us (0.37)
  blocking collectives: 40.2 us -> 0 us
  Pallas kernels: 0 us -> 36.1 us
  waiting for transfers between devices: 30.3 us -> 0 us
  starting transfers between devices: 15.3 us -> 0 us
  between operations: 14.4 us -> 0.64 us
  other arithmetic: 8.27 us -> 0 us
  matrix products: 6.88 us -> 0 us
    pallas_call x0 -> x1, Pallas kernels: none -> 36.1 us  [shards(): pl.pallas_call(functools.partial(kernel, ep_n, tp_n), out_shape=(jax.Shap...]
    reduce_scatter x1 -> x0, waiting for transfers between devices: 17.4 us -> none  [shards(): lax.psum_scatter(partial_value.astype(jnp.bfloat16), 'tp', scatter_dimens...]
    all_gather x3 -> x0, blocking collectives: 17.2 us -> none  [the longest x1 6.14 us: shards(): lax.all_gather(q_part, 'tp', axis=1, tiled=True)]
    all_to_all x4 -> x0, starting transfers between devices: 15.3 us -> none  [the longest x1 5.52 us: shards(): lax.all_to_all(reduced, 'ep', split_axis=1, concat_axis=0, tiled=True)]
    all_to_all x4 -> x0, waiting for transfers between devices: 12.9 us -> none  [the longest x1 6.2 us: shards(): lax.all_to_all(reduced, 'ep', split_axis=1, concat_axis=0, tiled=True)]
    all_to_all x1 -> x0, blocking collectives: 12.8 us -> none  [shards(): lax.all_to_all(buffer.reshape(experts_all, capacity, own_cols.shape[1]),...]
    psum x1 -> x0, blocking collectives: 10.3 us -> none  [shards(): lax.psum(jnp.dot(head_values, attn_out, preferred_element_type=jnp.float3...]
    dot_general x14 -> x0, matrix products: 6.88 us -> none  [the longest x1 1.19 us: shards(): jnp.dot(normed, q_down, preferred_element_type=jnp.float32)]
  transfers between devices with their start and end apart: 5 -> 0, of which waited for: 4 -> 0; matrix products, arithmetic and copies ran while one was open for 7% -> 0% of each run, Pallas kernels for 0% -> 0%
where the time goes in v1:
time: 47.1 us; the launch traced here: 46.7 us
  Pallas kernels  36.1 us (77%)
  local copies, waits for them, and re-layouts  9.98 us (21%)
  between operations  0.64 us (1%)
    pallas_call x1, Pallas kernels, shards(): pl.pallas_call(functools.partial(kernel, ep_n, tp_n), out_shape=(jax.Shap...  36.1 us
    unnamed x7, local copies, waits for them, and re-layouts  9.98 us

profile of v1, /device:TPU:0, one launch (start us, length us, event | category | flops | bytes accessed | tf_op | source)
XLA Modules:
  0.0 46.7 jit_solution(4188124857968850078)
XLA Ops:
  0.6 1.4 %copy.26.route = s32[16,6]{1,0:T(8,128)} copy(s32[16,6]{0,1:T(8,128)} %param.37) | data formatting | bytes 768 | tf_op args[16]
  2.0 1.4 %copy.27.route_weight = f32[16,6]{1,0:T(8,128)} copy(f32[16,6]{0,1:T(8,128)} %param.38) | data formatting | bytes 768 | tf_op args[17]
  3.3 1.7 %copy.24.rope_down_h = bf16[1024,32]{1,0:T(8,128)(2,1)} copy(bf16[1024,32]{0,1:T(8,128)(2,1)} %param.25) | data formatting | bytes 131072 | tf_op args[4]
  5.0 1.8 %copy.25.q_up_h = bf16[512,192]{1,0:T(8,128)(2,1)} copy(bf16[512,192]{0,1:T(8,128)(2,1)} %param.28) | data formatting | bytes 393216 | tf_op args[7]
  6.8 36.1 %shard_map.220 = (bf16[16,256]{1,0:T(8,128)(2,1)}, bf16[16,128]{1,0:T(8,128)(2,1)}, bf16[16,32]{1,0:T(8,128)(2,1)}) custom-call(bf16[16,1024]{1,0:T(8,128)(2,1)} %tokens.1, f32[1,1024]{1,0:T(1,128)} %bitcast.5, bf16[1024,128]{1,0:T(8,128)(2,1)} %q_down_h.1, bf16[1024,128]{1,0:T(8,128)(2,1)} %kv_down_h.1, bf16[1024,32]{1,0:T(8,128)(2,1)} %copy.24.rope_down_h, ...), custom_call_target="tpu_custom_call" | custom-call | tf_op jit(solution)/shard_map/pallas_call | solution.py:522
  42.9 1.3 %copy.31 = bf16[16,256]{1,0:T(8,128)(2,1)} copy(bf16[16,256]{1,0:T(8,128)(2,1)} %get-tuple-element.6) | data formatting | bytes 16384
  44.1 1.3 %copy.32 = bf16[16,128]{1,0:T(8,128)(2,1)} copy(bf16[16,128]{1,0:T(8,128)(2,1)} %get-tuple-element.7) | data formatting | bytes 8192
  45.4 1.3 %copy.33 = bf16[16,32]{1,0:T(8,128)(2,1)} copy(bf16[16,32]{1,0:T(8,128)(2,1)} %get-tuple-element.8) | data formatting | bytes 2048

commit v2 on v1

--- a/solution.py
+++ b/solution.py
@@ -46,65 +46,55 @@
     return jnp.dot(a, b, preferred_element_type=F32, precision=lax.Precision.HIGHEST)
 
 
-def kernel(
-    ep_n,
-    tp_n,
-    tokens,
-    attn_gain,
-    q_down_h,
-    kv_down_h,
-    rope_down_h,
-    q_gain,
-    kv_gain,
-    q_up_h,
-    query_gain,
-    key_up_h,
-    value_up_h,
-    attn_out_h,
-    cache_h,
-    rope_h,
-    lengths,
-    moe_gain,
-    route,
-    route_weight,
-    gate_h,
-    up_h,
-    down_h,
-    mixed_ref,
-    latent_ref,
-    rope_ref,
-    q_down,
-    kv_down,
-    rope_down,
-    q_up,
-    key_up,
-    value_up,
-    attn_out,
-    cache,
-    crope,
-    gate_w,
-    up_w,
-    down_w,
-    lat_buf,
-    query_out,
-    query_in,
-    att_out,
-    att_in,
-    sum_out,
-    sum_in,
-    rows_in,
-    part_out,
-    part_in,
-    load_sem,
-    tp_send,
-    tp_recv,
-    all_send,
-    all_recv,
-):
+def kernel(ep_n, tp_n, count, *refs):
+    far = refs[:count]
+    mixed_ref, latent_ref, rope_ref = refs[count : count + 3]
+    near = refs[count + 3 : 2 * count + 3]
+    (
+        tokens,
+        attn_gain,
+        q_down,
+        kv_down,
+        rope_down,
+        q_gain,
+        kv_gain,
+        q_up,
+        query_gain,
+        key_up,
+        value_up,
+        attn_out,
+        cache,
+        crope,
+        lengths,
+        moe_gain,
+        route,
+        route_weight,
+        gate_w,
+        up_w,
+        down_w,
+    ) = near
+    (
+        lat_buf,
+        query_out,
+        query_in,
+        att_out,
+        att_in,
+        sum_out,
+        sum_in,
+        rows_in,
+        part_out,
+        part_in,
+        back_out,
+        back_in,
+        load_sem,
+        tp_send,
+        tp_recv,
+        rows_recv,
+        part_recv,
+        bulk,
+    ) = refs[2 * count + 3 :]
     ep_me = lax.axis_index("ep")
     me = lax.axis_index("tp")
-    n = ep_n * tp_n
-    lin = ep_me * tp_n + me
     seqs = tokens.shape[0]
     cols = tokens.shape[1] // tp_n
     heads, qk = query_gain.shape
@@ -116,36 +106,19 @@
     block = heads * s_here
     lanes = 128
 
-    loads = [
-        pltpu.make_async_copy(src, dst, load_sem.at[i])
-        for i, (src, dst) in enumerate(
-            [
-                (q_down_h, q_down),
-                (kv_down_h, kv_down),
-                (rope_down_h, rope_down),
-                (q_up_h, q_up),
-                (key_up_h, key_up),
-                (rope_h, crope),
-                (cache_h, cache),
-                (value_up_h, value_up),
-                (attn_out_h, attn_out),
-                (gate_h, gate_w),
-                (up_h, up_w),
-                (down_h, down_w),
-            ]
-        )
-    ]
-    for load in loads:
-        load.start()
+    loads = [pltpu.make_async_copy(far[i], near[i], load_sem.at[i]) for i in range(count)]
+    for i in (0, 1, 2, 3, 4, 14, 5, 6, 7, 8, 9, 13, 12, 10, 11, 15, 16, 17, 18, 19, 20):
+        loads[i].start()
 
     barrier = pltpu.get_barrier_semaphore()
+    for k in range(1, tp_n):
+        pl.semaphore_signal(barrier, inc=1, device_id=(ep_me, lax.rem(me + k, tp_n)), device_id_type=MESH)
 
     def greet(k, carry):
-        to = lax.rem(lin + k, n)
-        pl.semaphore_signal(barrier, inc=1, device_id=(to // tp_n, lax.rem(to, tp_n)), device_id_type=MESH)
+        pl.semaphore_signal(barrier, inc=1, device_id=(lax.rem(ep_me + k, ep_n), me), device_id_type=MESH)
         return carry
 
-    lax.fori_loop(1, n, greet, 0)
+    lax.fori_loop(1, ep_n, greet, 0)
 
     def tp_copy(stage, src, dst, to, origin):
         return pltpu.make_async_remote_copy(
@@ -172,23 +145,26 @@
             other = lax.rem(me + k, tp_n)
             tp_copy(stage, src_of(other), dst_of(other), other, other).wait_send()
 
+    loads[0].wait()
+    loads[1].wait()
     tok = tokens[...].astype(F32)
     normed = (tok * lax.rsqrt(jnp.mean(tok * tok, axis=-1, keepdims=True) + EPS) * attn_gain[...]).astype(BF)
-    loads[0].wait()
+    loads[2].wait()
     qc = q_down.shape[1]
     kc = kv_down.shape[1]
     q_part = mm(normed, q_down[...]).astype(BF)
-    loads[1].wait()
+    loads[3].wait()
     kv_part = mm(normed, kv_down[...]).astype(BF)
     lat_buf[me, :, :qc] = q_part
     lat_buf[me, :, qc:] = kv_part
-    pl.semaphore_wait(barrier, n - 1)
+    pl.semaphore_wait(barrier, ep_n + tp_n - 2)
     own_lat = lambda to: lat_buf.at[me]
     lat_at = lambda i: lat_buf.at[i]
     exchange(0, own_lat, lat_at)
 
-    loads[2].wait()
-    new_rope = mm(normed, rope_down[...]).astype(BF)
+    loads[4].wait()
+    loads[14].wait()
+    new_rope = mm_nt(normed, rope_down[...]).astype(BF)
     rope_ref[...] = new_rope
     len_row = lengths[...].astype(F32)
     eye = iota((seqs, seqs), 0) == iota((seqs, seqs), 1)
@@ -219,6 +195,7 @@
     tile = jnp.zeros((qk, width), F32)
     for h in range(heads):
         tile = jnp.where(g_c - h * qk == g_i, 1.0, tile)
+    loads[8].wait()
     gains = exact(query_gain[...], tile)
     lane_w = iota((1, width), 1)
     gain = gains[0:1]
@@ -235,7 +212,7 @@
     head_lanes = div(lane_l, NOPE) == row_head
     rope_lanes = div(lane_l, ropes) == row_head
 
-    loads[5].wait()
+    loads[13].wait()
     positions = crope.shape[2]
     inv_sub = jnp.exp(iota((half, positions), 0).astype(F32) * (-math.log(ROPE_BASE) / half))
     kang = inv_sub * iota((half, positions), 1).astype(F32)
@@ -252,9 +229,10 @@
     arrive(0, own_lat, lat_at)
     q_raw = jnp.concatenate([lat_buf[t, :, :qc] for t in range(tp_n)], axis=1).astype(F32)
     kv_raw = jnp.concatenate([lat_buf[t, :, qc:] for t in range(tp_n)], axis=1).astype(F32)
+    loads[5].wait()
     q_lat = (q_raw * lax.rsqrt(jnp.mean(q_raw * q_raw, axis=-1, keepdims=True) + EPS) * q_gain[...]).astype(BF)
-    loads[3].wait()
-    query = mm(q_lat, q_up[...])
+    loads[7].wait()
+    query = mm_nt(q_lat, q_up[...])
     scale = jnp.zeros_like(query)
     lane_q = iota(query.shape, 1)
     for h in range(heads):
@@ -266,7 +244,7 @@
     rot = (exact(query, pick_a) * cos_q + exact(query, pick_b) * sin_q).astype(BF)
     nope_rows = jnp.where(head_lanes, mm(spread, nope), 0.0).astype(BF)
     rot_rows = jnp.where(rope_lanes, mm(spread, rot), 0.0).astype(BF)
-    loads[4].wait()
+    loads[9].wait()
     absorbed = mm_nt(nope_rows, key_up[...]).astype(BF)
     for t in range(tp_n):
         query_out[t, :, :rank] = absorbed[t * block : (t + 1) * block]
@@ -277,12 +255,13 @@
     query_in[me] = query_out[me]
 
     kv_scale = lax.rsqrt(jnp.mean(kv_raw * kv_raw, axis=-1, keepdims=True) + EPS)
+    loads[6].wait()
     latent_new = (kv_raw * kv_scale * kv_gain[...]).astype(BF)
     own_cols = pl.ds(pl.multiple_of(me * kc, kc), kc)
     latent_ref[...] = (kv_part.astype(F32) * kv_scale * kv_gain[:, own_cols]).astype(BF)
     latent_rows = mm(mine, latent_new)
     key_rows = mm(mine, key_new)
-    loads[6].wait()
+    loads[12].wait()
 
     arrive(1, q_src, q_dst)
     q_abs = jnp.concatenate([query_in[t, :, :rank] for t in range(tp_n)], axis=0)
@@ -314,8 +293,8 @@
     a_dst = lambda i: att_in.at[i]
     exchange(2, a_src, a_dst)
     att_in[me] = att_out[me]
-    loads[7].wait()
-    loads[8].wait()
+    loads[10].wait()
+    loads[11].wait()
     seq_i, row_c = iota((seqs, rows), 0), iota((seqs, rows), 1)
     gather = jnp.where(div(row_c, block) * s_here + mod(row_c, s_here) == seq_i, 1.0, 0.0).astype(BF)
 
@@ -332,39 +311,65 @@
     sum_in[me] = sum_out[me]
     model_cols = pl.ds(pl.multiple_of(me * cols, cols), cols)
     tok_mine = tokens[:, model_cols].astype(F32)
-    loads[9].wait()
-    loads[10].wait()
-    loads[11].wait()
+    for i in (15, 16, 17, 18, 19, 20):
+        loads[i].wait()
+    eye_row = lambda row: jnp.sum(jnp.where(eye, row, 0.0), axis=1, keepdims=True)
+    topk = route.shape[0]
+    chosen = [eye_row(route[k : k + 1, :].astype(F32)) for k in range(topk)]
+    chosen_weight = [eye_row(route_weight[k : k + 1, :]) for k in range(topk)]
 
     arrive(3, s_src, s_dst)
     head_sum = sum_in[0].astype(F32)
     for t in range(1, tp_n):
         head_sum = head_sum + sum_in[t].astype(F32)
     resid = (tok_mine + head_sum).astype(BF)
-    rows_in[lin] = resid
-
-    def all_copy(stage, src, dst, to):
+    rows_in[me, ep_me] = resid
+
+    def rows_copy(origin, to):
         return pltpu.make_async_remote_copy(
-            src_ref=src,
-            dst_ref=dst,
-            send_sem=all_send.at[stage],
-            recv_sem=all_recv.at[stage],
-            device_id=(to // tp_n, lax.rem(to, tp_n)),
+            src_ref=rows_in.at[me, origin],
+            dst_ref=rows_in.at[me, origin],
+            send_sem=bulk.at[0],
+            recv_sem=rows_recv.at[origin],
+            device_id=(to, me),
             device_id_type=MESH,
         )
 
+    def pass_on(origin):
+        for k in range(1, tp_n):
+            pltpu.make_async_remote_copy(
+                src_ref=rows_in.at[me, origin],
+                dst_ref=rows_in.at[me, origin],
+                send_sem=bulk.at[1],
+                recv_sem=bulk.at[2],
+                device_id=(ep_me, lax.rem(me + k, tp_n)),
+                device_id_type=MESH,
+            ).start()
+
+    def by_distance(k):
+        away = lax.div(k + 1, 2)
+        return lax.rem(jnp.where(lax.rem(k, 2) == 1, ep_me + away, ep_me + ep_n - away), ep_n)
+
     def give_rows(k, carry):
-        to = lax.rem(lin + k, n)
-        all_copy(0, rows_in.at[lin], rows_in.at[lin], to).start()
+        rows_copy(ep_me, by_distance(ep_n - k)).start()
         return carry
 
-    lax.fori_loop(1, n, give_rows, 0)
-
-    def all_wait(stage, src, dst):
-        others = pl.ds(0, n - 1)
-        return all_copy(stage, src.at[others], dst.at[others], lax.rem(lin + 1, n))
-
-    all_wait(0, rows_in, rows_in).wait_recv()
+    lax.fori_loop(1, ep_n, give_rows, 0)
+    pass_on(ep_me)
+
+    def take_rows(k, carry):
+        origin = by_distance(k)
+        rows_copy(origin, origin).wait_recv()
+        pass_on(origin)
+        return carry
+
+    lax.fori_loop(1, ep_n, take_rows, 0)
+
+    def bulk_wait(ref, sem):
+        return pltpu.make_async_copy(ref, ref, sem)
+
+    most = rows_in.at[pl.ds(0, tp_n - 1)]
+    bulk_wait(most, bulk.at[2]).wait()
 
     group = math.gcd(ep_n, 8)
 
@@ -373,7 +378,7 @@
         parts = []
         square = jnp.zeros((group * seqs, 1), F32)
         for t in range(tp_n):
-            x = jnp.concatenate([rows_in[(first + i) * tp_n + t] for i in range(group)], axis=0).astype(F32)
+            x = jnp.concatenate([rows_in[t, first + i] for i in range(group)], axis=0).astype(F32)
             square = square + jnp.sum(x * x, axis=-1, keepdims=True)
             parts.append(x)
         inverse = lax.rsqrt(square * (1.0 / (cols * tp_n)) + EPS)
@@ -389,7 +394,7 @@
             here = slice(t * cols, (t + 1) * cols)
             part = mm(hidden, down_w[0, :, here]).astype(BF)
             for i in range(group):
-                part_out[(first + i) * tp_n + t] = part[i * seqs : (i + 1) * seqs]
+                part_out[t, first + i] = part[i * seqs : (i + 1) * seqs]
         return carry
 
     if ep_n == group:
@@ -397,38 +402,84 @@
     else:
         lax.fori_loop(0, ep_n // group, expert, 0)
 
+    def part_copy(to_tp, block_ep, origin):
+        return pltpu.make_async_remote_copy(
+            src_ref=part_out.at[to_tp, block_ep],
+            dst_ref=part_in.at[origin, block_ep],
+            send_sem=bulk.at[3],
+            recv_sem=part_recv.at[block_ep, origin],
+            device_id=(ep_me, to_tp),
+            device_id_type=MESH,
+        )
+
     def give_parts(k, carry):
-        to = lax.rem(lin + k, n)
-        all_copy(1, part_out.at[to], part_in.at[lin], to).start()
+        block_ep = by_distance(ep_n - k)
+        for j in range(1, tp_n):
+            part_copy(lax.rem(me + j, tp_n), block_ep, me).start()
         return carry
 
-    lax.fori_loop(1, n, give_parts, 0)
-    part_in[lin] = part_out[lin]
-    chosen = route[...]
-    chosen_weight = route_weight[...]
-    all_wait(1, part_out, part_in).wait_recv()
-
-    def combine(e, mixed):
-        found = part_in[e * tp_n].astype(F32)
-        for t in range(1, tp_n):
-            found = found + part_in[e * tp_n + t].astype(F32)
-        share = jnp.sum(jnp.where(chosen == e, chosen_weight, 0.0), axis=1, keepdims=True)
-        return mixed + share * found.astype(BF).astype(F32)
-
+    lax.fori_loop(1, ep_n + 1, give_parts, 0)
+
+    def back_copy(to):
+        return pltpu.make_async_remote_copy(
+            src_ref=back_out.at[to],
+            dst_ref=back_in.at[ep_me],
+            send_sem=bulk.at[4],
+            recv_sem=bulk.at[5],
+            device_id=(to, me),
+            device_id_type=MESH,
+        )
+
+    def summed(block_ep):
+        found = part_out[me, block_ep].astype(F32)
+        for j in range(1, tp_n):
+            origin = lax.rem(me + j, tp_n)
+            part_copy(origin, block_ep, origin).wait_recv()
+            found = found + part_in[origin, block_ep].astype(F32)
+        return found.astype(BF)
+
+    def give_back(k, carry):
+        to = by_distance(ep_n - k)
+        back_out[to] = summed(to)
+        back_copy(to).start()
+        return carry
+
+    lax.fori_loop(1, ep_n, give_back, 0)
+    back_in[ep_me] = summed(ep_me)
+
+    def share_of(e):
+        share = jnp.zeros((seqs, 1), F32)
+        for k in range(topk):
+            share = share + jnp.where(chosen[k] == jnp.float32(e), chosen_weight[k], 0.0)
+        return share
+
+    few = ep_n <= 8
+    shares = [share_of(e) for e in range(ep_n)] if few else None
+    bulk_wait(back_in.at[pl.ds(0, ep_n - 1)], bulk.at[5]).wait()
     mixed = jnp.zeros((seqs, cols), F32)
-    if ep_n <= 8:
+    if few:
         for e in range(ep_n):
-            mixed = combine(e, mixed)
+            mixed = mixed + shares[e] * back_in[e].astype(F32)
     else:
-        mixed = lax.fori_loop(0, ep_n, combine, mixed)
+        mixed = lax.fori_loop(
+            0, ep_n, lambda e, m: m + share_of(lax.convert_element_type(e, F32)) * back_in[e].astype(F32), mixed
+        )
     mixed_ref[...] = (resid.astype(F32) + mixed).astype(BF)
 
     sent(0, own_lat, lat_at)
     sent(1, q_src, q_dst)
     sent(2, a_src, a_dst)
     sent(3, s_src, s_dst)
-    all_wait(0, rows_in, rows_in).wait_send()
-    all_wait(1, part_out, part_in).wait_send()
+    bulk_wait(back_out.at[pl.ds(0, ep_n - 1)], bulk.at[0]).wait()
+    bulk_wait(most, bulk.at[1]).wait()
+    bulk_wait(most, bulk.at[3]).wait()
+    bulk_wait(back_out.at[pl.ds(0, ep_n - 1)], bulk.at[4]).wait()
+
+
+def finish(a, b, c, x, y, z):
+    x[...] = a[...]
+    y[...] = b[...]
+    z[...] = c[...]
 
 
 def shards(ep_n, tp_n, *args):
@@ -462,10 +513,10 @@
         row(attn_gain),
         q_down,
         kv_down,
-        rope_down,
+        rope_down.T,
         row(q_latent_gain),
         row(kv_latent_gain),
-        q_up,
+        q_up.T,
         query_gain,
         key_up,
         value_up,
@@ -474,15 +525,14 @@
         cache_rope,
         row(lengths),
         row(moe_gain),
-        route,
-        route_weight,
+        route.T,
+        route_weight.T,
         expert_gate,
         expert_up,
         expert_down,
     )
-    far = {2, 3, 4, 7, 9, 10, 11, 12, 13, 18, 19, 20}
     vmem = pl.BlockSpec(memory_space=pltpu.VMEM)
-    anyspace = pl.BlockSpec(memory_space=pl.ANY)
+    anyspace = pl.BlockSpec(memory_space=pltpu.HBM)
     seqs, model = tokens.shape
     cols = model // tp_n
     n = ep_n * tp_n
@@ -490,19 +540,7 @@
     s_here, _, rank = cache_latent.shape
     block = heads * s_here
     like = lambda v: pltpu.VMEM(v.shape, v.dtype)
-    scratch = [
-        like(q_down),
-        like(kv_down),
-        like(rope_down),
-        like(q_up),
-        like(key_up),
-        like(value_up),
-        like(attn_out),
-        like(cache_latent),
-        like(cache_rope),
-        like(expert_gate),
-        like(expert_up),
-        like(expert_down),
+    scratch = [like(v) for v in operands] + [
         pltpu.VMEM((tp_n, seqs, q_down.shape[1] + kv_down.shape[1]), BF),
         pltpu.VMEM((tp_n, block, rank + 128), BF),
         pltpu.VMEM((tp_n, block, rank + 128), BF),
@@ -510,29 +548,33 @@
         pltpu.VMEM((tp_n, block, rank), BF),
         pltpu.VMEM((tp_n, seqs, cols), BF),
         pltpu.VMEM((tp_n, seqs, cols), BF),
-        pltpu.VMEM((n, seqs, cols), BF),
-        pltpu.VMEM((n, seqs, cols), BF),
-        pltpu.VMEM((n, seqs, cols), BF),
-        pltpu.SemaphoreType.DMA((12,)),
+        pltpu.VMEM((tp_n, ep_n, seqs, cols), BF),
+        pltpu.VMEM((tp_n, ep_n, seqs, cols), BF),
+        pltpu.VMEM((tp_n, ep_n, seqs, cols), BF),
+        pltpu.VMEM((ep_n, seqs, cols), BF),
+        pltpu.VMEM((ep_n, seqs, cols), BF),
+        pltpu.SemaphoreType.DMA((len(operands),)),
         pltpu.SemaphoreType.DMA((4, tp_n)),
         pltpu.SemaphoreType.DMA((4, tp_n)),
-        pltpu.SemaphoreType.DMA((2,)),
-        pltpu.SemaphoreType.DMA((2,)),
+        pltpu.SemaphoreType.DMA((ep_n,)),
+        pltpu.SemaphoreType.DMA((ep_n, tp_n)),
+        pltpu.SemaphoreType.DMA((6,)),
     ]
-    return pl.pallas_call(
-        functools.partial(kernel, ep_n, tp_n),
-        out_shape=(
-            jax.ShapeDtypeStruct((seqs, cols), BF),
-            jax.ShapeDtypeStruct((seqs, kv_down.shape[1]), BF),
-            jax.ShapeDtypeStruct((seqs, rope_down.shape[1]), BF),
-        ),
-        in_specs=[anyspace if i in far else vmem for i in range(len(operands))],
+    outs = (
+        jax.ShapeDtypeStruct((seqs, cols), BF),
+        jax.ShapeDtypeStruct((seqs, kv_down.shape[1]), BF),
+        jax.ShapeDtypeStruct((seqs, rope_down.shape[1]), BF),
+    )
+    grant = 60 * 1024 * 1024
+    found = pl.pallas_call(
+        functools.partial(kernel, ep_n, tp_n, len(operands)),
+        out_shape=outs,
+        in_specs=[anyspace] * len(operands),
         out_specs=(vmem, vmem, vmem),
         scratch_shapes=scratch,
-        compiler_params=pltpu.CompilerParams(
-            collective_id=0, has_side_effects=True, vmem_limit_bytes=60 * 1024 * 1024
-        ),
+        compiler_params=pltpu.CompilerParams(collective_id=0, has_side_effects=True, vmem_limit_bytes=grant),
     )(*operands)
+    return pl.pallas_call(finish, out_shape=outs, in_specs=[vmem] * 3, out_specs=(vmem, vmem, vmem), compiler_params=pltpu.CompilerParams(vmem_limit_bytes=1024 * 1024))(*found)
 
 
 def solution(mesh):

time: 47.1 us -> 41.7 us (0.89)
  local copies, waits for them, and re-layouts: 9.98 us -> 2.05 us
  Pallas kernels: 36.1 us -> 38.7 us
    unnamed x7 -> x6, local copies, waits for them, and re-layouts: 9.98 us -> 2.05 us
    pallas_call x1 -> x2, Pallas kernels: 36.1 us -> 38.7 us  [the longest x1 38.1 us: shards(): pl.pallas_call(functools.partial(kernel, ep_n, tp_n, len(operands)), out_...]
where the time goes in v2:
time: 41.7 us; the launch traced here: 41.4 us
  Pallas kernels  38.7 us (93%)
  local copies, waits for them, and re-layouts  2.05 us (5%)
  between operations  0.66 us (2%)
    pallas_call x1, Pallas kernels, shards(): pl.pallas_call(functools.partial(kernel, ep_n, tp_n, len(operands)), out_...  38.1 us
    unnamed x6, local copies, waits for them, and re-layouts  2.05 us

profile of v2, /device:TPU:0, one launch (start us, length us, event | category | flops | bytes accessed | tf_op | source)
XLA Modules:
  0.0 41.4 jit_solution(1451443796973083592)
XLA Ops:
  0.6 38.1 %shard_map.220 = (bf16[16,256]{1,0:T(8,128)(2,1)}, bf16[16,128]{1,0:T(8,128)(2,1)}, bf16[16,32]{1,0:T(8,128)(2,1)}) custom-call(bf16[16,1024]{1,0:T(8,128)(2,1)} %refs_0_.1, f32[1,1024]{1,0:T(1,128)} %bitcast.11, bf16[1024,128]{1,0:T(8,128)(2,1)} %refs_2_.1, bf16[1024,128]{1,0:T(8,128)(2,1)} %refs_3_.1, bf16[32,1024]{1,0:T(8,128)(2,1)} %bitcast.10, ...), custom_call_target="tpu_custom_call" | custom-call | tf_op jit(solution)/shard_map/pallas_call | solution.py:569
  38.7 0.0 copy-start
  38.7 0.7 %copy-done = bf16[16,256]{1,0:T(8,128)(2,1)S(1)} copy-done((bf16[16,256]{1,0:T(8,128)(2,1)S(1)}, bf16[16,256]{1,0:T(8,128)(2,1)}, u32[]{:S(2)}) %copy-start) | copy-done | bytes 8216
  39.4 0.0 copy-start.1
  39.4 0.7 %copy-done.1 = bf16[16,128]{1,0:T(8,128)(2,1)S(1)} copy-done((bf16[16,128]{1,0:T(8,128)(2,1)S(1)}, bf16[16,128]{1,0:T(8,128)(2,1)}, u32[]{:S(2)}) %copy-start.1) | copy-done | bytes 4120
  40.1 0.0 copy-start.2
  40.1 0.7 %copy-done.2 = bf16[16,32]{1,0:T(8,128)(2,1)S(1)} copy-done((bf16[16,32]{1,0:T(8,128)(2,1)S(1)}, bf16[16,32]{1,0:T(8,128)(2,1)}, u32[]{:S(2)}) %copy-start.2) | copy-done | bytes 1048
  40.8 0.6 %shard_map.221 = (bf16[16,256]{1,0:T(8,128)(2,1)}, bf16[16,128]{1,0:T(8,128)(2,1)}, bf16[16,32]{1,0:T(8,128)(2,1)}) custom-call(bf16[16,256]{1,0:T(8,128)(2,1)S(1)} %copy-done, bf16[16,128]{1,0:T(8,128)(2,1)S(1)} %copy-done.1, bf16[16,32]{1,0:T(8,128)(2,1)S(1)} %copy-done.2), custom_call_target="tpu_custom_call" | custom-call | tf_op jit(solution)/shard_map/pallas_call | solution.py:577
Async XLA Ops:
  38.7 0.7 %copy-start = (bf16[16,256]{1,0:T(8,128)(2,1)S(1)}, bf16[16,256]{1,0:T(8,128)(2,1)}, u32[]{:S(2)}) copy-start(bf16[16,256]{1,0:T(8,128)(2,1)} %get-tuple-element.6.a) | copy-start | bytes 24580
  39.4 0.7 %copy-start.1 = (bf16[16,128]{1,0:T(8,128)(2,1)S(1)}, bf16[16,128]{1,0:T(8,128)(2,1)}, u32[]{:S(2)}) copy-start(bf16[16,128]{1,0:T(8,128)(2,1)} %get-tuple-element.7.b) | copy-start | bytes 12292
  40.1 0.7 %copy-start.2 = (bf16[16,32]{1,0:T(8,128)(2,1)S(1)}, bf16[16,32]{1,0:T(8,128)(2,1)}, u32[]{:S(2)}) copy-start(bf16[16,32]{1,0:T(8,128)(2,1)} %get-tuple-element.8.c) | copy-start | bytes 3076

commit v3 on v2

--- a/solution.py
+++ b/solution.py
@@ -92,6 +92,7 @@
         rows_recv,
         part_recv,
         bulk,
+        near_sem,
     ) = refs[2 * count + 3 :]
     ep_me = lax.axis_index("ep")
     me = lax.axis_index("tp")
@@ -114,11 +115,35 @@
     for k in range(1, tp_n):
         pl.semaphore_signal(barrier, inc=1, device_id=(ep_me, lax.rem(me + k, tp_n)), device_id_type=MESH)
 
-    def greet(k, carry):
-        pl.semaphore_signal(barrier, inc=1, device_id=(lax.rem(ep_me + k, ep_n), me), device_id_type=MESH)
-        return carry
-
-    lax.fori_loop(1, ep_n, greet, 0)
+    pair, pairs = ep_me // 2, ep_n // 2
+    sides = (
+        (pair >= 0, ep_me + 1 - 2 * lax.rem(ep_me, 2), 0),
+        (pair > 0, ep_me - 2, 2),
+        (pair < pairs - 1, ep_me + 2, 1),
+    )
+
+    def each_side(act):
+        for slot, (there, peer, seen) in enumerate(sides):
+
+            @pl.when(there)
+            def _():
+                act(slot, peer, seen)
+
+    each_side(
+        lambda slot, peer, seen: pl.semaphore_signal(
+            barrier, inc=1, device_id=(peer, me), device_id_type=MESH
+        )
+    )
+
+    def tell():
+        each_side(
+            lambda slot, peer, seen: pl.semaphore_signal(
+                near_sem.at[seen], inc=1, device_id=(peer, me), device_id_type=MESH
+            )
+        )
+
+    def hear():
+        each_side(lambda slot, peer, seen: pl.semaphore_wait(near_sem.at[slot], 1))
 
     def tp_copy(stage, src, dst, to, origin):
         return pltpu.make_async_remote_copy(
@@ -157,10 +182,12 @@
     kv_part = mm(normed, kv_down[...]).astype(BF)
     lat_buf[me, :, :qc] = q_part
     lat_buf[me, :, qc:] = kv_part
-    pl.semaphore_wait(barrier, ep_n + tp_n - 2)
+    pl.semaphore_wait(barrier, tp_n + jnp.where(pair > 0, 1, 0) + jnp.where(pair < pairs - 1, 1, 0))
     own_lat = lambda to: lat_buf.at[me]
     lat_at = lambda i: lat_buf.at[i]
     exchange(0, own_lat, lat_at)
+    if pairs > 1:
+        tell()
 
     loads[4].wait()
     loads[14].wait()
@@ -253,6 +280,9 @@
     q_dst = lambda i: query_in.at[i]
     exchange(1, q_src, q_dst)
     query_in[me] = query_out[me]
+    if pairs > 2:
+        hear()
+        tell()
 
     kv_scale = lax.rsqrt(jnp.mean(kv_raw * kv_raw, axis=-1, keepdims=True) + EPS)
     loads[6].wait()
@@ -293,6 +323,13 @@
     a_dst = lambda i: att_in.at[i]
     exchange(2, a_src, a_dst)
     att_in[me] = att_out[me]
+
+    def next_round(k, carry):
+        hear()
+        tell()
+        return carry
+
+    lax.fori_loop(2, pairs - 1, next_round, 0)
     loads[10].wait()
     loads[11].wait()
     seq_i, row_c = iota((seqs, rows), 0), iota((seqs, rows), 1)
@@ -309,6 +346,8 @@
     s_dst = lambda i: sum_in.at[i]
     exchange(3, s_src, s_dst)
     sum_in[me] = sum_out[me]
+    if pairs > 1:
+        hear()
     model_cols = pl.ds(pl.multiple_of(me * cols, cols), cols)
     tok_mine = tokens[:, model_cols].astype(F32)
     for i in (15, 16, 17, 18, 19, 20):
@@ -346,24 +385,37 @@
                 device_id_type=MESH,
             ).start()
 
-    def by_distance(k):
-        away = lax.div(k + 1, 2)
-        return lax.rem(jnp.where(lax.rem(k, 2) == 1, ep_me + away, ep_me + ep_n - away), ep_n)
-
-    def give_rows(k, carry):
-        rows_copy(ep_me, by_distance(ep_n - k)).start()
-        return carry
-
-    lax.fori_loop(1, ep_n, give_rows, 0)
+    def at_distance(d, act):
+        @pl.when(ep_me + d < ep_n)
+        def _():
+            act(ep_me + d)
+
+        @pl.when(ep_me >= d)
+        def _():
+            act(ep_me - d)
+
+    def farthest_first(act):
+        def step(k, carry):
+            at_distance(ep_n - k, act)
+            return carry
+
+        lax.fori_loop(1, ep_n, step, 0)
+
+    def nearest_first(act):
+        def step(k, carry):
+            at_distance(k, act)
+            return carry
+
+        lax.fori_loop(1, ep_n, step, 0)
+
+    farthest_first(lambda to: rows_copy(ep_me, to).start())
     pass_on(ep_me)
 
-    def take_rows(k, carry):
-        origin = by_distance(k)
+    def take_rows(origin):
         rows_copy(origin, origin).wait_recv()
         pass_on(origin)
-        return carry
-
-    lax.fori_loop(1, ep_n, take_rows, 0)
+
+    nearest_first(take_rows)
 
     def bulk_wait(ref, sem):
         return pltpu.make_async_copy(ref, ref, sem)
@@ -412,13 +464,12 @@
             device_id_type=MESH,
         )
 
-    def give_parts(k, carry):
-        block_ep = by_distance(ep_n - k)
+    def give_parts(block_ep):
         for j in range(1, tp_n):
             part_copy(lax.rem(me + j, tp_n), block_ep, me).start()
-        return carry
-
-    lax.fori_loop(1, ep_n + 1, give_parts, 0)
+
+    farthest_first(give_parts)
+    give_parts(ep_me)
 
     def back_copy(to):
         return pltpu.make_async_remote_copy(
@@ -438,13 +489,11 @@
             found = found + part_in[origin, block_ep].astype(F32)
         return found.astype(BF)
 
-    def give_back(k, carry):
-        to = by_distance(ep_n - k)
+    def give_back(to):
         back_out[to] = summed(to)
         back_copy(to).start()
-        return carry
-
-    lax.fori_loop(1, ep_n, give_back, 0)
+
+    farthest_first(give_back)
     back_in[ep_me] = summed(ep_me)
 
     def share_of(e):
@@ -506,7 +555,7 @@
         expert_up,
         expert_down,
     ) = args
-    assert expert_gate.shape[0] == 1
+    assert expert_gate.shape[0] == 1 and ep_n % 2 == 0
     row = lambda v: v.reshape(1, -1)
     operands = (
         tokens,
@@ -559,6 +608,7 @@
         pltpu.SemaphoreType.DMA((ep_n,)),
         pltpu.SemaphoreType.DMA((ep_n, tp_n)),
         pltpu.SemaphoreType.DMA((6,)),
+        pltpu.SemaphoreType.REGULAR((3,)),
     ]
     outs = (
         jax.ShapeDtypeStruct((seqs, cols), BF),
@@ -574,7 +624,7 @@
         scratch_shapes=scratch,
         compiler_params=pltpu.CompilerParams(collective_id=0, has_side_effects=True, vmem_limit_bytes=grant),
     )(*operands)
-    return pl.pallas_call(finish, out_shape=outs, in_specs=[vmem] * 3, out_specs=(vmem, vmem, vmem), compiler_params=pltpu.CompilerParams(vmem_limit_bytes=1024 * 1024))(*found)
+    return pl.pallas_call(finish, out_shape=outs, in_specs=[vmem] * 3, out_specs=(vmem, vmem, vmem), compiler_params=pltpu.CompilerParams(vmem_limit_bytes=grant))(*found)
 
 
 def solution(mesh):

time: 41.7 us -> 36.3 us (0.87)
  Pallas kernels: 38.7 us -> 35.5 us
  local copies, waits for them, and re-layouts: 2.05 us -> 0 us
    pallas_call x1, Pallas kernels: 38.1 us -> 34.2 us  [shards(): pl.pallas_call(functools.partial(kernel, ep_n, tp_n, len(operands)), out_...]
    unnamed x6 -> x0, local copies, waits for them, and re-layouts: 2.05 us -> none
    pallas_call x1, Pallas kernels: 0.61 us -> 1.31 us  [shards(): pl.pallas_call(finish, out_shape=outs, in_specs=[vmem] * 3, out_specs=(vm...]
where the time goes in v3:
time: 36.3 us; the launch traced here: 36.2 us
  Pallas kernels  35.5 us (98%)
  between operations  0.65 us (2%)
    pallas_call x1, Pallas kernels, shards(): pl.pallas_call(functools.partial(kernel, ep_n, tp_n, len(operands)), out_...  34.2 us
    pallas_call x1, Pallas kernels, shards(): pl.pallas_call(finish, out_shape=outs, in_specs=[vmem] * 3, out_specs=(vm...  1.31 us

profile of v3, /device:TPU:0, one launch (start us, length us, event | category | flops | bytes accessed | tf_op | source)
XLA Modules:
  0.0 36.2 jit_solution(16190620006759628364)
XLA Ops:
  0.6 34.2 %shard_map.220 = (bf16[16,256]{1,0:T(8,128)(2,1)}, bf16[16,128]{1,0:T(8,128)(2,1)}, bf16[16,32]{1,0:T(8,128)(2,1)}) custom-call(bf16[16,1024]{1,0:T(8,128)(2,1)} %refs_0_.1, f32[1,1024]{1,0:T(1,128)} %bitcast.11, bf16[1024,128]{1,0:T(8,128)(2,1)} %refs_2_.1, bf16[1024,128]{1,0:T(8,128)(2,1)} %refs_3_.1, bf16[32,1024]{1,0:T(8,128)(2,1)} %bitcast.10, ...), custom_call_target="tpu_custom_call" | custom-call | tf_op jit(solution)/shard_map/pallas_call | solution.py:619
  34.8 1.3 %shard_map.221 = (bf16[16,256]{1,0:T(8,128)(2,1)}, bf16[16,128]{1,0:T(8,128)(2,1)}, bf16[16,32]{1,0:T(8,128)(2,1)}) custom-call(bf16[16,256]{1,0:T(8,128)(2,1)} %get-tuple-element.6.a, bf16[16,128]{1,0:T(8,128)(2,1)} %get-tuple-element.7.b, bf16[16,32]{1,0:T(8,128)(2,1)} %get-tuple-element.8.c), custom_call_target="tpu_custom_call" | custom-call | tf_op jit(solution)/shard_map/pallas_call | solution.py:627

commit v4 on v3

--- a/solution.py
+++ b/solution.py
@@ -374,14 +374,17 @@
             device_id_type=MESH,
         )
 
+    low = lax.rem(me, 2)
+    peers = [lax.rem(me - low + i, tp_n) for i in range(2, tp_n)] + [me + 1 - 2 * low]
+
     def pass_on(origin):
-        for k in range(1, tp_n):
+        for peer in peers:
             pltpu.make_async_remote_copy(
                 src_ref=rows_in.at[me, origin],
                 dst_ref=rows_in.at[me, origin],
                 send_sem=bulk.at[1],
                 recv_sem=bulk.at[2],
-                device_id=(ep_me, lax.rem(me + k, tp_n)),
+                device_id=(ep_me, peer),
                 device_id_type=MESH,
             ).start()
 
@@ -465,8 +468,8 @@
         )
 
     def give_parts(block_ep):
-        for j in range(1, tp_n):
-            part_copy(lax.rem(me + j, tp_n), block_ep, me).start()
+        for peer in peers:
+            part_copy(peer, block_ep, me).start()
 
     farthest_first(give_parts)
     give_parts(ep_me)
@@ -555,7 +558,7 @@
         expert_up,
         expert_down,
     ) = args
-    assert expert_gate.shape[0] == 1 and ep_n % 2 == 0
+    assert expert_gate.shape[0] == 1 and ep_n % 2 == 0 and tp_n % 2 == 0
     row = lambda v: v.reshape(1, -1)
     operands = (
         tokens,

time: 36.3 us -> 36.3 us (level)
  no operation moved by 1% of the time
where the time goes in v4:
time: 36.3 us; the launch traced here: 36.2 us
  Pallas kernels  35.5 us (98%)
  between operations  0.65 us (2%)
    pallas_call x1, Pallas kernels, shards(): pl.pallas_call(functools.partial(kernel, ep_n, tp_n, len(operands)), out_...  34.2 us
    pallas_call x1, Pallas kernels, shards(): pl.pallas_call(finish, out_shape=outs, in_specs=[vmem] * 3, out_specs=(vm...  1.31 us

profile of v4, /device:TPU:0, one launch (start us, length us, event | category | flops | bytes accessed | tf_op | source)
XLA Modules:
  0.0 36.2 jit_solution(11762195296324464538)
XLA Ops:
  0.6 34.2 %shard_map.220 = (bf16[16,256]{1,0:T(8,128)(2,1)}, bf16[16,128]{1,0:T(8,128)(2,1)}, bf16[16,32]{1,0:T(8,128)(2,1)}) custom-call(bf16[16,1024]{1,0:T(8,128)(2,1)} %refs_0_.1, f32[1,1024]{1,0:T(1,128)} %bitcast.11, bf16[1024,128]{1,0:T(8,128)(2,1)} %refs_2_.1, bf16[1024,128]{1,0:T(8,128)(2,1)} %refs_3_.1, bf16[32,1024]{1,0:T(8,128)(2,1)} %bitcast.10, ...), custom_call_target="tpu_custom_call" | custom-call | tf_op jit(solution)/shard_map/pallas_call | solution.py:622
  34.8 1.3 %shard_map.221 = (bf16[16,256]{1,0:T(8,128)(2,1)}, bf16[16,128]{1,0:T(8,128)(2,1)}, bf16[16,32]{1,0:T(8,128)(2,1)}) custom-call(bf16[16,256]{1,0:T(8,128)(2,1)} %get-tuple-element.6.a, bf16[16,128]{1,0:T(8,128)(2,1)} %get-tuple-element.7.b, bf16[16,32]{1,0:T(8,128)(2,1)} %get-tuple-element.8.c), custom_call_target="tpu_custom_call" | custom-call | tf_op jit(solution)/shard_map/pallas_call | solution.py:630
